TPU v7x, 768 devices: a whole 4x8x12 slice. The times are simulated.
768 devices in a mesh: ep: 48 (over z, x), tp: 16 (over y, core).
Axes of the slice: x: 4, y: 8, z: 12, core: 2. Of those that a mesh axis runs over, the one named last changes fastest.
Arguments:
- tokens: bfloat16 [1536, 4096], P('ep'), may hold values from -6 to 6
- routes: int32 [1536, 4], P('ep'), may hold values from 0 to 47, all different within a row; in each aligned block of 32 rows (0 to 31, 32 to 63, ...) at most 4 rows name the same one
- mix_weights: float32 [1536, 4], P('ep'), may hold values from 0.2 to 1
- pre_gain: float32 [4096], replicated, may hold values from 0.1 to 1.9
- gate_weight: bfloat16 [48, 4096, 2048], P('ep', None, 'tp'), may hold values from -0.09375 to 0.09375
- up_weight: bfloat16 [48, 4096, 2048], P('ep', None, 'tp'), may hold values from -0.09375 to 0.09375
- down_weight: bfloat16 [48, 2048, 4096], P('ep', 'tp'), may hold values from -1 to 1
- post_gain: float32 [4096], P('tp'), may hold values from 0.1 to 1.9
Outputs:
- layer_out: bfloat16 [1536, 4096], P('ep', 'tp')
Inputs may be any that keep to these rules, and one draw needn't show every extreme that they name: `routes`: within a row the 4 experts differ; among the rows of one index of ep no expert is named more than 4 times.
All inputs are finite; a program needn't handle non-finite values.
Results may differ from a plain program's by a relative error of at most 0.019.
Values may be sent and summed in bfloat16 or wider, within the bound.
A program may use at most 32 MiB of HBM per device.

v0:
```python
import jax
import jax.numpy as jnp
from jax import lax
from jax.sharding import PartitionSpec as P

epsilon = 1e-06


def sent_to_all(shard, axis):
    copies = jnp.broadcast_to(shard, (lax.axis_size(axis), *shard.shape))
    return lax.all_to_all(copies, axis, split_axis=0, concat_axis=0, tiled=True)


def in_order(tiles, dim):
    tiles = jnp.moveaxis(tiles, 0, dim)
    dims = tiles.shape
    return tiles.reshape(*dims[:dim], dims[dim] * dims[dim + 1], *dims[dim + 2 :])


def gather_directly(shard, axis, dim):
    tiles = sent_to_all(shard, axis)
    return in_order(tiles, dim)


def in_blocks(shard, dim, count):
    before, after = (shard.shape[:dim], shard.shape[dim + 1 :])
    return jnp.moveaxis(shard.reshape(*before, count, -1, *after), dim, 0)


def summed_on_arrival(shard, axis, dim):
    count = lax.axis_size(axis)
    tiles = lax.all_to_all(in_blocks(shard, dim, count), axis, 0, 0, tiled=True)
    return jnp.sum(tiles.astype(jnp.float32), axis=0)


def of_everyone(shard, axis):
    return sent_to_all(shard, axis).sum(axis=0)


def on_device(
    tokens, routes, mix_weights, pre_gain, gate_weight, up_weight, down_weight, post_gain
):
    tok_rows, width = tokens.shape
    top_count = routes.shape[1]
    experts = lax.axis_size("ep")
    capacity = min(tok_rows, max(2, (3 * tok_rows * top_count + 2 * experts - 1) // (2 * experts)))
    floats = tokens.astype(jnp.float32)
    normed = (
        floats * lax.rsqrt(jnp.mean(floats * floats, axis=-1, keepdims=True) + epsilon) * pre_gain
    ).astype(jnp.bfloat16)
    chosen = routes.reshape(-1)
    onehot = (chosen[:, None] == jnp.arange(experts, dtype=jnp.int32)[None, :]).astype(jnp.int32)
    before = jnp.cumsum(onehot, axis=0) - onehot
    slot_rank = jnp.sum(before * onehot, axis=1)
    target = chosen * capacity + slot_rank
    placed = target[:, None] == jnp.arange(experts * capacity, dtype=jnp.int32)[None, :]
    by_choice = placed.reshape(tok_rows, top_count, experts * capacity)
    picked = jnp.any(by_choice, axis=1).astype(jnp.bfloat16)
    outgoing = jnp.einsum("tc,td->cd", picked, normed, preferred_element_type=jnp.float32).astype(
        jnp.bfloat16
    )
    outgoing = outgoing.reshape(experts, capacity, width)
    slice_width = width // lax.axis_size("tp")
    outgoing_part = lax.dynamic_slice_in_dim(
        outgoing, lax.axis_index("tp") * slice_width, slice_width, 2
    )
    arrived = lax.all_to_all(outgoing_part, "ep", split_axis=0, concat_axis=0, tiled=True)
    arrived = gather_directly(arrived, "tp", 2)
    arrived_rows = arrived.reshape(experts * capacity, width)
    gate_act = jnp.dot(arrived_rows, gate_weight[0], preferred_element_type=jnp.float32)
    up_act = jnp.dot(arrived_rows, up_weight[0], preferred_element_type=jnp.float32)
    hidden = (jax.nn.silu(gate_act) * up_act).astype(jnp.bfloat16)
    partial_value = jnp.dot(hidden, down_weight[0], preferred_element_type=jnp.float32)
    summed = summed_on_arrival(partial_value.astype(jnp.bfloat16), "tp", 1).astype(jnp.bfloat16)
    returned = lax.all_to_all(
        summed.reshape(experts, capacity, summed.shape[1]),
        "ep",
        split_axis=0,
        concat_axis=0,
        tiled=True,
    )
    results = returned.reshape(experts * capacity, summed.shape[1]).astype(jnp.float32)
    mixing = jnp.sum(mix_weights[:, :, None] * by_choice.astype(jnp.float32), axis=1)
    mixed = jnp.dot(mixing, results, precision=lax.Precision.HIGHEST)
    squares = jnp.sum(mixed * mixed, axis=1)
    total = of_everyone(squares, "tp")
    scale = lax.rsqrt(total / width + epsilon)
    return (mixed * scale[:, None] * post_gain).astype(jnp.bfloat16)


def solution(mesh):
    in_specs = (
        P("ep", None),
        P("ep", None),
        P("ep", None),
        P(),
        P("ep", None, "tp"),
        P("ep", None, "tp"),
        P("ep", "tp", None),
        P("tp"),
    )
    out_specs = P("ep", "tp")
    return jax.shard_map(
        on_device, mesh=mesh, in_specs=in_specs, out_specs=out_specs, check_vma=False
    )
```

profile of v0, /device:TPU:1, one launch (start us, length us, event | category | flops | bytes accessed | tf_op | source)
XLA Modules:
  0.0 168.6 jit_solution(3522528377016615358)
XLA Ops:
  0.0 0.0 copy-start
  0.0 0.9 copy.36
  0.9 0.1 eq.29
  1.0 0.1 fusion.18
  1.1 0.2 reduce_window_sum.11
  1.2 0.2 select_reduce_fusion.1
  1.4 0.1 reduce_sum.60
  1.5 0.1 copy.37
  1.6 0.7 multiply_add_fusion
  2.3 0.1 fusion.12
  2.4 1.1 fusion.6
  3.5 1.6 convolution_convert_fusion.1
  5.1 2.0 %reshape.51 = bf16[48,4,4096]{2,1,0:T(4,128)(2,1)} reshape(bf16[192,4096]{1,0:T(8,128)(2,1)S(1)} %convolution_convert_fusion.1) | data formatting | bytes 3145728 | tf_op jit(solution)/shard_map/reshape | solution.py:62
  7.1 0.9 constant_dynamic-slice_fusion
  8.1 30.0 %all_to_all.26 = bf16[48,4,256]{2,1,0:T(4,128)(2,1)S(1)} all-to-all(bf16[48,4,256]{2,1,0:T(4,128)(2,1)S(1)} %constant_dynamic-slice_fusion), channel_id=1, replica_groups=mesh['ep'=48,'tp'=16] {'ep'}, dimensions={0} | all-to-all | bytes 196608 | tf_op jit(solution)/shard_map/all_to_all | solution.py:67
  38.1 0.6 broadcast_in_dim.4
  38.7 49.3 %all_to_all.27 = bf16[16,48,4,256]{3,2,1,0:T(4,128)(2,1)S(1)} all-to-all(bf16[16,48,4,256]{3,2,1,0:T(4,128)(2,1)S(1)} %broadcast_in_dim.4), channel_id=1, replica_groups=mesh['ep'=48,'tp'=16] {'tp'}, dimensions={0} | all-to-all | bytes 3145728 | tf_op jit(solution)/shard_map/all_to_all | solution.py:11
  88.0 1.7 copy.38
  89.6 0.0 copy-start.1
  89.7 0.7 copy.42
  90.4 0.5 copy-done.1
  90.9 0.6 fusion.4
  91.5 0.0 copy-done
  91.5 3.4 %convolution_convert_fusion = bf16[192,4096]{1,0:T(8,128)(2,1)} fusion(bf16[192,4096]{1,0:T(8,128)(2,1)S(1)} %bitcast.28, bf16[1,128,4096]{2,1,0:T(8,128)(2,1)S(1)} %copy-done, bf16[1,4096,128]{2,1,0:T(8,128)(2,1)} %param.13, f32[192,128]{1,0:T(8,128)S(1)} %fusion.4), kind=kOutput, calls=%fused_computation | convolution fusion | flops 403587072 | bytes 5341184 | tf_op jit(solution)/shard_map/dot_general | solution.py:73
  94.9 1.6 copy.44
  96.5 42.5 %all_to_all.28 = bf16[16,192,256]{2,1,0:T(8,128)(2,1)S(1)} all-to-all(bf16[16,192,256]{2,1,0:T(8,128)(2,1)S(1)} %bitcast.31), channel_id=1, replica_groups=mesh['ep'=48,'tp'=16] {'tp'}, dimensions={0} | all-to-all | bytes 3145728 | tf_op jit(solution)/shard_map/all_to_all | solution.py:32
  138.9 0.0 copy-start.2
  138.9 0.0 copy-start.3
  138.9 0.2 reduce_sum.63
  139.2 0.7 reshape.53
  139.8 4.5 %all-to-all-start.3 = ((bf16[48,4,256]{2,1,0:T(4,128)(2,1)}), bf16[48,4,256]{2,1,0:T(4,128)(2,1)S(1)}, u32[]{:S(2)}, u32[]{:S(2)}) async-start(bf16[48,4,256]{2,1,0:T(4,128)(2,1)} %reshape.53), calls=%async_computation.3 | async-start | bytes 196608 | tf_op jit(solution)/shard_map/all_to_all | solution.py:75
  144.3 0.0 copy-done.2
  144.3 0.1 select_reduce_fusion
  144.5 12.3 %all-to-all-done.3 = bf16[48,4,256]{2,1,0:T(4,128)(2,1)S(1)} async-done(((bf16[48,4,256]{2,1,0:T(4,128)(2,1)}), bf16[48,4,256]{2,1,0:T(4,128)(2,1)S(1)}, u32[]{:S(2)}, u32[]{:S(2)}) %all-to-all-start.3) | async-done | bytes 98336 | tf_op jit(solution)/shard_map/all_to_all | solution.py:75
  156.7 0.3 multiply_reduce_fusion
  157.0 10.8 %all_to_all.29 = f32[16,1,32]{2,1,0:T(1,128)S(1)} all-to-all(f32[16,1,32]{2,1,0:T(1,128)S(1)} %broadcast_in_dim.5), channel_id=1, replica_groups=mesh['ep'=48,'tp'=16] {'tp'}, dimensions={0} | all-to-all | bytes 4096 | tf_op jit(solution)/shard_map/all_to_all | solution.py:11
  167.9 0.0 copy-done.3
  167.9 0.7 multiply_convert_fusion
  (5 shorter events, 0.1 us)
Async XLA Ops:
  0.0 91.5 %copy-start = (bf16[1,128,4096]{2,1,0:T(8,128)(2,1)S(1)}, bf16[1,128,4096]{2,1,0:T(8,128)(2,1)}, u32[]{:S(2)}) copy-start(bf16[1,128,4096]{2,1,0:T(8,128)(2,1)} %param.14) | copy-start | bytes 3145732
  89.6 1.2 copy-start.1
  138.9 5.4 %copy-start.2 = (f32[32,4]{0,1:T(4,128)S(1)}, f32[32,4]{0,1:T(4,128)}, u32[]{:S(2)}) copy-start(f32[32,4]{0,1:T(4,128)} %param.10) | copy-start | bytes 1540
  138.9 29.0 %copy-start.3 = (f32[256]{0:T(256)S(1)}, f32[256]{0:T(256)}, u32[]{:S(2)}) copy-start(f32[256]{0:T(256)} %param.15) | copy-start | bytes 3076
  139.8 16.9 %all-to-all-start.3 = ((bf16[48,4,256]{2,1,0:T(4,128)(2,1)}), bf16[48,4,256]{2,1,0:T(4,128)(2,1)S(1)}, u32[]{:S(2)}, u32[]{:S(2)}) async-start(bf16[48,4,256]{2,1,0:T(4,128)(2,1)} %reshape.53), calls=%async_computation.3 | async-start | bytes 196608 | tf_op jit(solution)/shard_map/all_to_all | solution.py:75
where the time goes:
time: 169 us
  blocking collectives  133 us (79%)
  waiting for transfers between devices  12.3 us (7%)
  local copies, waits for them, and re-layouts  9.84 us (6%)
  matrix products  5.9 us (3%)
  starting transfers between devices  4.52 us (3%)
  other arithmetic  3.36 us (2%)
    all_to_all x2, blocking collectives, sent_to_all(): return lax.all_to_all(copies, axis, split_axis=0, concat_axis=0, tiled=True)  60.1 us
    all_to_all x1, blocking collectives, summed_on_arrival(): tiles = lax.all_to_all(in_blocks(shard, dim, count), axis, 0, 0, tiled=True)  42.5 us
    all_to_all x1, blocking collectives, on_device(): lax.all_to_all(outgoing_part, 'ep', split_axis=0, concat_axis=0, tiled=True)  30 us
    all_to_all x1, waiting for transfers between devices, on_device(): lax.all_to_all(summed.reshape(experts, capacity, summed.shape[1]), 'ep',...  12.3 us
    all_to_all x1, starting transfers between devices, on_device(): lax.all_to_all(summed.reshape(experts, capacity, summed.shape[1]), 'ep',...  4.52 us
    dot_general x1, matrix products, on_device(): jnp.dot(hidden, down_weight[0], preferred_element_type=jnp.float32)  3.44 us
  transfers between devices with their start and end apart: 1, of which 1 were waited for; matrix products, arithmetic and copies ran while one was open for 0% of the time, Pallas kernels for 0%

commit v1 on v0

v1 whole, which is shorter than its diff:
```python
import functools

import jax
import jax.numpy as jnp
from jax import lax
from jax.experimental import pallas as pl
from jax.experimental.pallas import tpu as pltpu
from jax.sharding import PartitionSpec as P

EPS = 1e-06
CAP = 4
QUARTER = 128
X_CHIPS = 4
CORES = 2
bf16, f32, i32 = jnp.bfloat16, jnp.float32, jnp.int32


def one_hot(shape, match):
    rows = lax.broadcasted_iota(i32, shape, 0)
    cols = lax.broadcasted_iota(i32, shape, 1)
    return jnp.where(match(rows, cols), 1.0, 0.0).astype(bf16)


def kernel(
    z_chips,
    x_chips,
    y_chips,
    tokens,
    routes,
    mix_weights,
    pre_gain,
    gate_weight,
    up_weight,
    down_weight,
    post_gain,
    out,
    tok,
    rts,
    mix,
    gain,
    pgain,
    wgu,
    wd,
    bt,
    mx,
    stack,
    outgoing,
    incoming,
    xf,
    acc,
    fstack,
    send_r,
    send_l,
    recv_r,
    recv_l,
    back_out,
    back_in,
    mixed,
    theirs,
    ss,
    load_sem,
    weight_sem,
    weight_send,
    weight_recv,
    out_sem,
    in_sem,
    gr_send,
    gl_send,
    gather_sem,
    sr_send,
    sl_send,
    rr_sem,
    rl_sem,
    back_send,
    back_recv,
    half_send,
    half_recv,
    ss_send,
    ss_recv,
):
    rows, width = tok.shape
    count = z_chips * x_chips // CORES
    per = count // 2
    block = width // y_chips
    quarters = block // QUARTER
    tile = quarters * CAP
    group = per * CAP
    units = wd.shape[0] // CORES
    hops = y_chips // 2
    half_x = x_chips // 2
    lanes = count * tile

    ep, tp = lax.axis_index("ep"), lax.axis_index("tp")
    z, x = ep // x_chips, ep % x_chips
    y, c = tp // CORES, tp % CORES
    partner = {"tp": y * CORES + (1 - c)}
    right = {"tp": ((y + 1) % y_chips) * CORES + c}
    left = {"tp": ((y + y_chips - 1) % y_chips) * CORES + c}

    def offset(k):
        step = k // half_x
        dz = jnp.where(step % 2 == 1, (step + 1) // 2, z_chips - step // 2) % z_chips
        return dz, c + CORES * (k % half_x)

    def ahead(k):
        dz, dx = offset(k)
        return {"ep": ((z + dz) % z_chips) * x_chips + (x + dx) % x_chips}

    def behind(k):
        dz, dx = offset(k)
        return {
            "ep": ((z + z_chips - dz) % z_chips) * x_chips + (x + x_chips - dx) % x_chips
        }

    def remote(src, dst, send, recv, device):
        return pltpu.make_async_remote_copy(
            src_ref=src,
            dst_ref=dst,
            send_sem=send,
            recv_sem=recv,
            device_id=device,
            device_id_type=pl.DeviceIdType.MESH,
        )

    barrier = pltpu.get_barrier_semaphore()

    def greet_ep(k, carry):
        @pl.when((k > 0) | (c > 0))
        def _():
            pl.semaphore_signal(
                barrier, 1, device_id=behind(k), device_id_type=pl.DeviceIdType.MESH
            )

        return carry

    def greet_tp(k, carry):
        pl.semaphore_signal(
            barrier,
            1,
            device_id={"tp": (tp + k) % (y_chips * CORES)},
            device_id_type=pl.DeviceIdType.MESH,
        )
        return carry

    lax.fori_loop(0, count, greet_ep, 0)
    lax.fori_loop(1, y_chips * CORES, greet_tp, 0)

    loads = [
        pltpu.make_async_copy(tokens, tok, load_sem.at[0]),
        pltpu.make_async_copy(routes, rts, load_sem.at[1]),
        pltpu.make_async_copy(mix_weights, mix, load_sem.at[2]),
        pltpu.make_async_copy(pre_gain, gain, load_sem.at[3]),
        pltpu.make_async_copy(post_gain, pgain, load_sem.at[4]),
    ]
    for load in loads:
        load.start()

    own_units = pl.multiple_of(c * units, units)
    gate_slot = wgu.at[:, pl.ds(own_units, units)]
    up_slot = wgu.at[:, pl.ds(pl.multiple_of((CORES + c) * units, units), units)]
    down_slot = wd.at[pl.ds(own_units, units), :]
    weights = [
        (gate_weight.at[0], gate_slot),
        (up_weight.at[0], up_slot),
        (down_weight.at[0], down_slot),
    ]
    own_weights = [
        pltpu.make_async_copy(src, dst, weight_sem.at[n]) for n, (src, dst) in enumerate(weights)
    ]
    for load in own_weights:
        load.start()
    for load in loads:
        load.wait()

    shape = (rows, lanes)
    col = lax.broadcasted_iota(i32, shape, 1)
    col_k, col_q, col_slot = col // tile, (col // CAP) % quarters, col % CAP
    dz, dx = offset(col_k)
    expert = ((z + dz) % z_chips) * x_chips + (x + dx) % x_chips
    named = jnp.zeros(shape, f32)
    weight = jnp.zeros(shape, f32)
    square = lax.broadcasted_iota(i32, (rows, rows), 0) == lax.broadcasted_iota(
        i32, (rows, rows), 1
    )
    for k in range(rts.shape[0]):
        chosen = jnp.where(square, rts[k : k + 1, :].astype(f32), 0.0)
        hit = jnp.sum(chosen, axis=1, keepdims=True) == expert.astype(f32)
        share = jnp.where(square, mix[k : k + 1, :], 0.0)
        named += jnp.where(hit, 1.0, 0.0)
        weight += jnp.where(hit, jnp.sum(share, axis=1, keepdims=True), 0.0)
    earlier = one_hot((rows, rows), lambda r, s: s < r)
    rank = jnp.dot(earlier, named.astype(bf16), preferred_element_type=f32)
    placed = jnp.where((rank == col_slot.astype(f32)) & (named > 0.0), 1.0, 0.0)
    weight = weight * placed

    floats = tok[...].astype(f32)
    scale = lax.rsqrt(jnp.mean(floats * floats, axis=-1, keepdims=True) + EPS)
    for q in range(quarters):
        part = pl.ds(q * rows, rows)
        feats = pl.ds(pl.multiple_of(y * block + q * QUARTER, QUARTER), QUARTER)
        stack[part, :] = (tok[:, feats].astype(f32) * scale * gain[:, feats]).astype(bf16)
        bt[part, :] = jnp.where(col_q == q, placed, 0.0).astype(bf16)
        w = jnp.where(col_q == q, weight, 0.0)
        high = w.astype(bf16)
        mx[part, :] = high
        mx[pl.ds((quarters + q) * rows, rows), :] = (w - high.astype(f32)).astype(bf16)
    outgoing[...] = (
        lax.dot_general(
            bt[...], stack[...], (((0,), (0,)), ((), ())), preferred_element_type=f32
        )
        .astype(bf16)
        .reshape(outgoing.shape)
    )

    waited = y_chips * CORES - 1 + count - jnp.where(c == 0, 1, 0)
    pl.semaphore_wait(barrier, waited)

    def dispatch(k, carry):
        own = (k == 0) & (c == 0)
        g = k // per

        @pl.when(own)
        def _():
            copy = pltpu.make_async_copy(outgoing.at[0], incoming.at[0], in_sem.at[0])
            copy.start()

        @pl.when(jnp.logical_not(own))
        def _():
            remote(outgoing.at[k], incoming.at[k], out_sem, in_sem.at[g], ahead(k)).start()

        return carry

    lax.fori_loop(0, count, dispatch, 0)

    sent_weights = [
        remote(src, dst, weight_send.at[n], weight_recv.at[n], partner)
        for n, (src, dst) in enumerate(weights)
    ]
    for copy in sent_weights:
        copy.start()

    size = per * tile
    sort = one_hot(
        (size, size),
        lambda r, s: (
            (s // tile == (r // CAP) % per)
            & ((s // CAP) % quarters == r // group)
            & (s % CAP == r % CAP)
        ),
    )
    unsort = one_hot(
        (size, size),
        lambda s, r: (
            (s // tile == (r // CAP) % per)
            & ((s // CAP) % quarters == r // group)
            & (s % CAP == r % CAP)
        ),
    )

    def pass_right(d, h):
        return remote(
            xf.at[(y_chips - d) % y_chips, h],
            xf.at[y_chips - d - 1, h],
            gr_send.at[d, h],
            gather_sem.at[y_chips - d - 1, h],
            right,
        )

    def pass_left(d, h):
        return remote(
            xf.at[d, h], xf.at[d + 1, h], gl_send.at[d, h], gather_sem.at[d + 1, h], left
        )

    def goes_right(d, h):
        return d < hops - 1 or (d == hops - 1 and h == 0)

    def goes_left(d, h):
        return d < hops - 1 or (d == hops - 1 and h == 1)

    for h in range(2):
        arrived = incoming.at[pl.ds(h * per, per)]
        pltpu.make_async_copy(arrived, arrived, in_sem.at[h]).wait()
        tiles = arrived[...].reshape(size, QUARTER)
        sorted_rows = jnp.dot(sort, tiles, preferred_element_type=f32).astype(bf16)
        for q in range(quarters):
            xf[0, h, :, q * QUARTER : (q + 1) * QUARTER] = sorted_rows[
                q * group : (q + 1) * group
            ]
        pass_right(0, h).start()
        pass_left(0, h).start()

    for load in own_weights:
        load.wait()
    for copy in sent_weights:
        copy.wait_recv()

    def product(o):
        depth = pl.ds(pl.multiple_of(((y + o) % y_chips) * block, block), block)
        return jnp.dot(
            xf[o].reshape(2 * group, block), wgu[depth, :], preferred_element_type=f32
        )

    acc[...] = product(0)
    for d in range(1, hops + 1):
        for h in range(2):
            if goes_right(d - 1, h):
                pass_right(d - 1, h).wait_recv()
                if goes_right(d, h):
                    pass_right(d, h).start()
            if goes_left(d - 1, h):
                pass_left(d - 1, h).wait_recv()
                if goes_left(d, h):
                    pass_left(d, h).start()
        if d < hops:
            acc[...] += product(y_chips - d) + product(d)
        else:
            acc[...] += product(d)

    gate, up = acc[:, : CORES * units], acc[:, CORES * units :]
    hidden = (gate / (1.0 + jnp.exp(-gate)) * up).astype(bf16)

    def partial(o):
        cols = pl.ds(pl.multiple_of(((y + o) % y_chips) * block, block), block)
        return jnp.dot(hidden, wd[:, cols], preferred_element_type=f32)

    def sum_right(s, h):
        return remote(
            send_r.at[s, h], recv_r.at[s - 1, h], sr_send.at[s, h], rr_sem.at[s - 1, h], right
        )

    def sum_left(s, h):
        return remote(
            send_l.at[s, h], recv_l.at[s - 1, h], sl_send.at[s, h], rl_sem.at[s - 1, h], left
        )

    last = partial(hops)
    send_r[hops, 0] = last[:group].astype(bf16)
    sum_right(hops, 0).start()
    send_l[hops, 1] = last[group:].astype(bf16)
    sum_left(hops, 1).start()
    for s in range(hops - 1, 0, -1):
        to_right, to_left = partial(s), partial(y_chips - s)
        for n in range(2):
            h = n if s < hops - 1 else 1 - n
            term = to_right[h * group : (h + 1) * group]
            if s < hops - 1 or h == 0:
                sum_right(s + 1, h).wait_recv()
                term += recv_r[s, h].astype(f32)
            send_r[s, h] = term.astype(bf16)
            sum_right(s, h).start()
            h = 1 - h
            term = to_left[h * group : (h + 1) * group]
            if s < hops - 1 or h == 1:
                sum_left(s + 1, h).wait_recv()
                term += recv_l[s, h].astype(f32)
            send_l[s, h] = term.astype(bf16)
            sum_left(s, h).start()

    own = partial(0)
    for h in range(2):
        sum_right(1, h).wait_recv()
        sum_left(1, h).wait_recv()
        total = (
            own[h * group : (h + 1) * group]
            + recv_r[0, h].astype(f32)
            + recv_l[0, h].astype(f32)
        ).astype(bf16)
        for q in range(quarters):
            fstack[h, q * group : (q + 1) * group, :] = total[:, q * QUARTER : (q + 1) * QUARTER]
        back_out[pl.ds(h * per, per)] = (
            jnp.dot(unsort, fstack[h], preferred_element_type=f32)
            .astype(bf16)
            .reshape(per, tile, QUARTER)
        )

        def give_back(k, carry, h=h):
            own = (k == 0) & (c == 0)

            @pl.when(own)
            def _():
                copy = pltpu.make_async_copy(back_out.at[k], back_in.at[k], back_recv.at[h])
                copy.start()

            @pl.when(jnp.logical_not(own))
            def _():
                remote(
                    back_out.at[k], back_in.at[k], back_send, back_recv.at[h], behind(k)
                ).start()

            return carry

        lax.fori_loop(h * per, (h + 1) * per, give_back, 0)

    total = jnp.zeros((2 * quarters * rows, QUARTER), f32)
    for h in range(2):
        arrived = back_in.at[pl.ds(h * per, per)]
        pltpu.make_async_copy(arrived, arrived, back_recv.at[h]).wait()
        total += jnp.dot(
            mx[:, h * size : (h + 1) * size],
            arrived[...].reshape(size, QUARTER),
            preferred_element_type=f32,
        )
    mixed[...] = total[: quarters * rows] + total[quarters * rows :]
    half = quarters * rows // CORES
    swap = remote(
        mixed.at[pl.ds(pl.multiple_of((1 - c) * half, half), half)],
        theirs,
        half_send,
        half_recv,
        partner,
    )
    swap.start()
    swap.wait_recv()
    final = mixed[pl.ds(pl.multiple_of(c * half, half), half), :] + theirs[...]
    final = final.reshape(quarters // CORES, rows, QUARTER)

    squares = jnp.sum(jnp.sum(final * final, axis=0), axis=-1, keepdims=True)
    diagonal = lax.broadcasted_iota(i32, (rows, QUARTER), 0) == lax.broadcasted_iota(
        i32, (rows, QUARTER), 1
    )
    ss[tp] = jnp.sum(jnp.where(diagonal, squares, 0.0), axis=0, keepdims=True)

    def tell(k, carry):
        remote(
            ss.at[tp], ss.at[tp], ss_send, ss_recv, {"tp": (tp + k) % (y_chips * CORES)}
        ).start()
        return carry

    lax.fori_loop(1, y_chips * CORES, tell, 0)
    others = ss.at[pl.ds(0, y_chips * CORES - 1)]
    pltpu.make_async_copy(others, others, ss_recv).wait()
    squares = jnp.sum(ss[...], axis=0)
    squares = jnp.sum(jnp.where(diagonal, squares, 0.0), axis=1, keepdims=True)
    scale = lax.rsqrt(squares / width + EPS)
    for q in range(quarters // CORES):
        cols = slice(q * QUARTER, (q + 1) * QUARTER)
        out[:, cols] = (final[q] * scale * pgain[:, cols]).astype(bf16)

    pltpu.make_async_copy(others, others, ss_send).wait()
    swap.wait_send()
    for copy in sent_weights:
        copy.wait_send()

    def sent(buffer, sem):
        @pl.when(c == 0)
        def _():
            most = buffer.at[pl.ds(1, count - 1)]
            pltpu.make_async_copy(most, most, sem).wait()

        @pl.when(c != 0)
        def _():
            pltpu.make_async_copy(buffer, buffer, sem).wait()

    sent(outgoing, out_sem)
    sent(back_out, back_send)
    for d in range(hops):
        for h in range(2):
            if goes_right(d, h):
                pass_right(d, h).wait_send()
                sum_right(d + 1, h).wait_send()
            if goes_left(d, h):
                pass_left(d, h).wait_send()
                sum_left(d + 1, h).wait_send()


def on_device(
    tokens, routes, mix_weights, pre_gain, gate_weight, up_weight, down_weight, post_gain
):
    rows, width = tokens.shape
    units = gate_weight.shape[2]
    experts, tps = lax.axis_size("ep"), lax.axis_size("tp")
    x_chips = min(X_CHIPS, experts // 2)
    z_chips, y_chips = experts // x_chips, tps // CORES
    count = experts // CORES
    block = width // y_chips
    quarters = block // QUARTER
    tile = quarters * CAP
    group = count // 2 * CAP
    hops = y_chips // 2
    vmem, dma = pltpu.VMEM, pltpu.SemaphoreType.DMA
    anywhere = pl.BlockSpec(memory_space=pl.ANY)
    ring = (hops + 1, 2, group, block)
    return pl.pallas_call(
        functools.partial(kernel, z_chips, x_chips, y_chips),
        out_shape=jax.ShapeDtypeStruct((rows, width // tps), bf16),
        in_specs=[anywhere] * 8,
        out_specs=pl.BlockSpec(memory_space=pltpu.VMEM),
        scratch_shapes=[
            vmem((rows, width), bf16),
            vmem(routes.shape[::-1], i32),
            vmem(mix_weights.shape[::-1], f32),
            vmem((1, width), f32),
            vmem((1, width // tps), f32),
            vmem((width, 2 * CORES * units), bf16),
            vmem((CORES * units, width), bf16),
            vmem((quarters * rows, count * tile), bf16),
            vmem((2 * quarters * rows, count * tile), bf16),
            vmem((quarters * rows, QUARTER), bf16),
            vmem((count, tile, QUARTER), bf16),
            vmem((count, tile, QUARTER), bf16),
            vmem((y_chips, 2, group, block), bf16),
            vmem((2 * group, 2 * CORES * units), f32),
            vmem((2, quarters * group, QUARTER), bf16),
            vmem(ring, bf16),
            vmem(ring, bf16),
            vmem(ring, bf16),
            vmem(ring, bf16),
            vmem((count, tile, QUARTER), bf16),
            vmem((count, tile, QUARTER), bf16),
            vmem((quarters * rows, QUARTER), f32),
            vmem((quarters * rows // CORES, QUARTER), f32),
            vmem((tps, 1, QUARTER), f32),
            dma((5,)),
            dma((3,)),
            dma((3,)),
            dma((3,)),
            dma,
            dma((2,)),
            dma((hops, 2)),
            dma((hops, 2)),
            dma((y_chips, 2)),
            dma((hops + 1, 2)),
            dma((hops + 1, 2)),
            dma((hops, 2)),
            dma((hops, 2)),
            dma,
            dma((2,)),
            dma,
            dma,
            dma,
            dma,
        ],
        compiler_params=pltpu.CompilerParams(collective_id=0, has_side_effects=True),
    )(
        tokens,
        routes.T,
        mix_weights.T,
        pre_gain.reshape(1, width),
        gate_weight,
        up_weight,
        down_weight,
        post_gain.reshape(1, width // tps),
    )


def solution(mesh):
    in_specs = (
        P("ep", None),
        P("ep", None),
        P("ep", None),
        P(),
        P("ep", None, "tp"),
        P("ep", None, "tp"),
        P("ep", "tp", None),
        P("tp"),
    )
    return jax.shard_map(
        on_device, mesh=mesh, in_specs=in_specs, out_specs=P("ep", "tp"), check_vma=False
    )
```

time: 169 us -> 75.9 us (0.45)
  blocking collectives: 133 us -> 0 us
  Pallas kernels: 0 us -> 74.4 us
  waiting for transfers between devices: 12.3 us -> 0 us
  local copies, waits for them, and re-layouts: 9.84 us -> 1.32 us
  matrix products: 5.9 us -> 0 us
  starting transfers between devices: 4.52 us -> 0 us
  other arithmetic: 3.36 us -> 0 us
    all_to_all x4 -> x0, blocking collectives: 133 us -> none  [the longest x2 60.1 us: sent_to_all(): return lax.all_to_all(copies, axis, split_axis=0, concat_axis=0, tiled=True)]
    pallas_call x0 -> x1, Pallas kernels: none -> 74.4 us  [on_device(): pl.pallas_call(functools.partial(kernel, z_chips, x_chips, y_chips), out_...]
    all_to_all x1 -> x0, waiting for transfers between devices: 12.3 us -> none  [on_device(): lax.all_to_all(summed.reshape(experts, capacity, summed.shape[1]), 'ep',...]
    dot_general x4 -> x0, matrix products: 5.9 us -> none  [the longest x1 3.44 us: on_device(): jnp.dot(hidden, down_weight[0], preferred_element_type=jnp.float32)]
    all_to_all x1 -> x0, starting transfers between devices: 4.52 us -> none  [on_device(): lax.all_to_all(summed.reshape(experts, capacity, summed.shape[1]), 'ep',...]
    reshape x4 -> x0, local copies, waits for them, and re-layouts: 4.25 us -> none  [the longest x1 2.01 us: on_device(): outgoing = outgoing.reshape(experts, capacity, width)]
  transfers between devices with their start and end apart: 1 -> 0, of which waited for: 1 -> 0; matrix products, arithmetic and copies ran while one was open for 0% -> 0% of each run, Pallas kernels for 0% -> 0%
where the time goes in v1:
time: 75.9 us; the launch traced here: 75.8 us
  Pallas kernels  74.4 us (98%)
  local copies, waits for them, and re-layouts  1.32 us (2%)
    pallas_call x1, Pallas kernels, on_device(): pl.pallas_call(functools.partial(kernel, z_chips, x_chips, y_chips), out_...  74.4 us

profile of v1, /device:TPU:1, one launch (start us, length us, event | category | flops | bytes accessed | tf_op | source)
XLA Modules:
  0.0 75.8 jit_solution(1638323119853245750)
XLA Ops:
  0.0 74.4 %shard_map.82 = bf16[32,256]{1,0:T(8,128)(2,1)} custom-call(bf16[32,4096]{1,0:T(8,128)(2,1)} %tokens.1, s32[4,32]{1,0:T(4,128)} %bitcast.5, f32[4,32]{1,0:T(4,128)} %bitcast.6, f32[1,4096]{1,0:T(1,128)} %bitcast.4, bf16[1,4096,128]{2,1,0:T(8,128)(2,1)} %gate_weight.1, bf16[1,4096,128]{2,1,0:T(8,128)(2,1)} %up_weight.1, bf16[1,128,4096]{2,1,0:T(8,128)(2,1)} %down_weight.1, ...), custom_call_target="tpu_custom_call" | custom-call | tf_op jit(solution)/shard_map/pallas_call | solution.py:483
  74.4 1.3 %copy.10 = bf16[32,256]{1,0:T(8,128)(2,1)} copy(bf16[32,256]{1,0:T(8,128)(2,1)} %shard_map.82) | data formatting | bytes 32768
